TPU v7x, 32 devices: a whole 2x2x4 slice. The times are simulated.
32 devices in a mesh: sp: 16 (over z, y, x), tp: 2 (over core).
Axes of the slice: x: 2, y: 2, z: 4, core: 2. Of those that a mesh axis runs over, the one named last changes fastest.
Arguments:
- query_rows: bfloat16 [4096, 1024], P('sp', 'tp'), may hold values from -6 to 6
- key_rows: bfloat16 [4096, 1024], P('sp', 'tp'), may hold values from -6 to 6
- value_rows: bfloat16 [4096, 1024], P('sp', 'tp'), may hold values from -6 to 6
- out_weight: bfloat16 [1024, 2048], P('tp'), may hold values from -0.75 to 0.75
Outputs:
- layer_out: bfloat16 [4096, 2048], P(('sp', 'tp'))
All inputs are finite; a program needn't handle non-finite values.
Results may differ from a plain program's by a relative error of at most 0.012.
Values may be sent and summed in bfloat16 or wider, within the bound.
A program may use at most 64 MiB of HBM per device.

v0:
```python
import functools
import math

import jax
import jax.numpy as jnp
import numpy as np
from jax import lax
from jax.experimental import pallas as pl
from jax.experimental.pallas import tpu as pltpu
from jax.sharding import PartitionSpec as P

HD = 64
BACK = 128
THETA = 500000.0
FAR = -1e30
F32 = jnp.float32
BF16 = jnp.bfloat16
LANES = 2 * HD
NT = (((1,), (1,)), ((), ()))


def place(p):
    return ((p & 7) << 4) + (((p >> 3) & 3) << 2) + (p >> 5)


def iota(shape, axis):
    return lax.broadcasted_iota(jnp.int32, shape, axis)


def kernel(
    G, ngroups, tp_count,
    q_hbm, k_hbm, v_hbm, cosb_hbm, sinb_hbm, inv_hbm, w_ref, out_ref,
    q_ref, k_ref, v_ref, cosb_ref, sinb_ref, inv_ref, qs, kvs, qr, kv, kvf, q2, q2f, acc, top, bias, wbuf, rs, rr, mx,
    s_kv, s_q, s_x, r_kv, r_q, r_x, w_sem, s_ret, r_ret, in_sem,
):
    loads = [
        pltpu.make_async_copy(source, dest, in_sem.at[n])
        for n, (source, dest) in enumerate((
            (inv_hbm, inv_ref), (cosb_hbm, cosb_ref), (sinb_hbm, sinb_ref),
            (k_hbm, k_ref), (v_hbm, v_ref), (q_hbm, q_ref),
        ))
    ]
    for load in loads:
        load.start()
    sp = lax.axis_index("sp")
    tp = lax.axis_index("tp")
    group = sp // G
    me = sp - group * G
    base = group * G
    has_prev = group > 0
    has_next = group < ngroups - 1
    seat = me * tp_count + tp
    seats = G * tp_count
    head = tp * G + me
    tok = q_ref.shape[0]
    halves = tok // BACK

    def target(s, t):
        return {"sp": s, "tp": t}

    barrier = pltpu.get_barrier_semaphore()
    for o in range(1, seats):
        n = lax.rem(seat + o, seats)
        pl.semaphore_signal(
            barrier, inc=1, device_id=target(base + n // tp_count, lax.rem(n, tp_count)),
            device_id_type=pl.DeviceIdType.MESH,
        )

    @pl.when(has_prev)
    def _():
        for o in range(G):
            pl.semaphore_signal(
                barrier, inc=1, device_id=target(base - G + o, tp),
                device_id_type=pl.DeviceIdType.MESH,
            )

    @pl.when(has_next)
    def _():
        for o in range(G):
            pl.semaphore_signal(
                barrier, inc=1, device_id=target(base + G + o, tp),
                device_id_type=pl.DeviceIdType.MESH,
            )

    w_local = pltpu.make_async_copy(w_ref, wbuf.at[tp], w_sem.at[0])
    w_local.start()

    for load in loads:
        load.wait()

    lane = iota((BACK, LANES), 1)
    low = lane < HD
    lane_t = iota((tok, LANES), 1)
    first = (lane_t & (HD - 1)) < HD // 2
    angle = inv_ref[...] * (sp * tok).astype(F32)
    ca = jnp.cos(angle)[:1]
    sa = jnp.sin(angle)[:1]
    cos = ca * cosb_ref[...] - sa * sinb_ref[...]
    sin = sa * cosb_ref[...] + ca * sinb_ref[...]
    sin = jnp.where(first, -sin, sin)
    swizzle = jnp.where(place(iota((BACK, BACK), 0)) == iota((BACK, BACK), 1), 1.0, 0.0).astype(BF16)
    back = jnp.where(place(iota((BACK, BACK), 1)) == iota((BACK, BACK), 0), 1.0, 0.0).astype(BF16)

    def turn(ref, cols):
        x = ref[:, cols].astype(F32)
        other = jnp.where(first, pltpu.roll(x, LANES - HD // 2, 1), pltpu.roll(x, HD // 2, 1))
        return (x * cos + other * sin).astype(BF16)

    def sw(x):
        return jnp.dot(swizzle, x, preferred_element_type=F32)

    for m in range(G // 2):
        cols = slice(m * LANES, (m + 1) * LANES)
        tq = turn(q_ref, cols)
        tk = turn(k_ref, cols)
        tv = v_ref[:, cols]
        qa = sw(tq[:BACK]) * (1.0 / math.sqrt(HD))
        qb = sw(tq[BACK:]) * (1.0 / math.sqrt(HD))
        qs[2 * m] = jnp.where(low, qa, pltpu.roll(qb, HD, 1)).astype(BF16)
        qs[2 * m + 1] = jnp.where(low, pltpu.roll(qa, HD, 1), qb).astype(BF16)
        for e in range(halves):
            ks = sw(tk[e * BACK : (e + 1) * BACK])
            vs = sw(tv[e * BACK : (e + 1) * BACK])
            kvs[2 * m, e] = jnp.where(low, ks, pltpu.roll(vs, HD, 1)).astype(BF16)
            kvs[2 * m + 1, e] = jnp.where(low, pltpu.roll(ks, HD, 1), vs).astype(BF16)

    pl.semaphore_wait(
        barrier, seats - 1 + jnp.where(has_prev, G, 0) + jnp.where(has_next, G, 0)
    )

    own0 = G * halves

    def copy_kv(dest):
        return pltpu.make_async_remote_copy(
            src_ref=kvs.at[dest], dst_ref=kv.at[pl.ds(own0 + halves * me, halves)],
            send_sem=s_kv.at[dest], recv_sem=r_kv.at[me],
            device_id=target(base + dest, tp), device_id_type=pl.DeviceIdType.MESH,
        )

    def copy_q(dest):
        return pltpu.make_async_remote_copy(
            src_ref=qs.at[dest], dst_ref=qr.at[me],
            send_sem=s_q.at[dest], recv_sem=r_q.at[me],
            device_id=target(base + dest, tp), device_id_type=pl.DeviceIdType.MESH,
        )

    def copy_x(dest):
        return pltpu.make_async_remote_copy(
            src_ref=kvs.at[dest], dst_ref=kv.at[pl.ds(halves * me, halves)],
            send_sem=s_x.at[dest], recv_sem=r_x.at[me],
            device_id=target(base + G + dest, tp), device_id_type=pl.DeviceIdType.MESH,
        )

    w_away = pltpu.make_async_remote_copy(
        src_ref=w_ref, dst_ref=wbuf.at[tp], send_sem=w_sem.at[1], recv_sem=w_sem.at[2],
        device_id=target(sp, tp_count - 1 - tp), device_id_type=pl.DeviceIdType.MESH,
    )

    bits = [1 << n for n in range(G.bit_length() - 1)]
    far = sorted(range(1, G), key=lambda o: -o.bit_count())

    def mate(o):
        return sum((((me // b + o // b) % 2) * b for b in bits), 0)

    for o in far:
        copy_kv(mate(o)).start()
        copy_q(mate(o)).start()

    @pl.when(has_next)
    def _():
        for o in range(G):
            copy_x(mate(o)).start()

    w_away.start()

    row = iota((BACK, 2 * BACK), 0)
    col = iota((BACK, 2 * BACK), 1)
    old = col < BACK
    missing = jnp.logical_and(old, group == 0)

    def stride4(n):
        w = n & 31
        return ((n >> 5) << 5) + ((w & 7) << 2) + (w >> 3)

    def masked(distance):
        return jnp.where((distance >= 0) & (distance <= BACK), 0.0, FAR)

    b1 = masked(place(row) + BACK - place(col & (BACK - 1)) - ((col >> 7) << 7))
    b4 = masked(stride4(row) + BACK - stride4(col))
    b16 = masked(row + BACK - col)
    bias[0] = b1
    bias[1] = b4
    bias[2] = jnp.where(missing, FAR, b1)
    bias[3] = jnp.where(missing, FAR, b4)
    bias[4] = jnp.where(missing, FAR, b16)

    acc[...] = jnp.zeros_like(acc)
    top[...] = jnp.full_like(top, FAR)

    @pl.when(jnp.logical_not(has_prev))
    def _():
        kv[:own0] = jnp.zeros((own0, BACK, LANES), BF16)

    kv[pl.ds(own0 + halves * me, halves)] = kvs[me]
    qr[me] = qs[me]

    def ready(s):
        x = qr[s].astype(F32)
        a = jnp.where(low, x, 0.0)
        b = jnp.where(low, pltpu.roll(x, HD, 1), 0.0)
        q2f[2 * s] = a
        q2f[2 * s + 1] = b
        q2[2 * s] = a.astype(BF16)
        q2[2 * s + 1] = b.astype(BF16)
        at = pl.ds(own0 + halves * s, halves)
        kvf[at] = kv[at].astype(F32)

    ready(me)
    for o in range(1, G):
        s = lax.rem(me - o + G, G)
        pltpu.make_async_remote_copy(
            src_ref=kvs.at[s], dst_ref=kv.at[pl.ds(own0 + halves * s, halves)],
            send_sem=s_kv.at[s], recv_sem=r_kv.at[s],
            device_id=target(base + s, tp), device_id_type=pl.DeviceIdType.MESH,
        ).wait_recv()
        pltpu.make_async_remote_copy(
            src_ref=qs.at[s], dst_ref=qr.at[s],
            send_sem=s_q.at[s], recv_sem=r_q.at[s],
            device_id=target(base + s, tp), device_id_type=pl.DeviceIdType.MESH,
        ).wait_recv()
        ready(s)

    low_keys = iota((2 * BACK, LANES), 1) < HD

    def attend(q, keys, b, o_old, t_old):
        s = lax.dot_general(q, keys, NT, preferred_element_type=F32) + b
        t_new = jnp.maximum(t_old, jnp.max(s, axis=1, keepdims=True))
        p = jnp.concatenate(
            [jnp.exp(s[:, :BACK] - t_new), jnp.exp(s[:, BACK:] - t_new)], axis=1
        ).astype(BF16)
        ones = jnp.where(low_keys, jnp.ones_like(keys), keys)
        o = jnp.dot(p, ones, preferred_element_type=F32)
        return o_old * jnp.exp(t_old - t_new) + o, t_new

    def run(tiles):
        done = []
        for q, keys, b, where in tiles:
            shape = acc[where].shape
            o, t = attend(
                q, keys, b, acc[where].reshape(BACK, LANES), top[where].reshape(BACK, LANES)
            )
            done.append((where, o.reshape(shape), t.reshape(shape)))
        for where, o, t in done:
            acc[where] = o
            top[where] = t

    def tile1(h, b):
        return (
            q2[h], kv[pl.ds(own0 - 1 + h, 2)].reshape(2 * BACK, LANES), bias[b], (h,),
        )

    def tile4(quarter, r, b):
        rows = pl.ds(r * 32, 32)
        return (
            q2[4 * quarter : 4 * quarter + 4, rows, :].reshape(BACK, LANES),
            kv[own0 + 4 * quarter - 4 : own0 + 4 * quarter + 4, rows, :].reshape(2 * BACK, LANES),
            bias[b],
            (slice(4 * quarter, 4 * quarter + 4), rows, slice(None)),
        )

    def tile16(r):
        rows = pl.ds(r * 8, 8)
        return (
            q2f[:, rows, :].reshape(BACK, LANES).astype(BF16),
            kvf[:, rows, :].reshape(2 * BACK, LANES).astype(BF16),
            bias[4],
            (slice(None), rows, slice(None)),
        )

    nq = G * halves

    @pl.loop(0, (nq - 1) // 3)
    def _(i):
        run([tile1(1 + 3 * i + n, 0) for n in range(3)])

    @pl.loop(0, 4)
    def _(r):
        run([tile4(n, r, 1) for n in range(1, nq // 4)])

    def arrive(sources):
        @pl.when(has_prev)
        def _():
            for s in sources:
                at = pl.ds(halves * s, halves)
                pltpu.make_async_remote_copy(
                    src_ref=kvs.at[s], dst_ref=kv.at[at], send_sem=s_x.at[s], recv_sem=r_x.at[s],
                    device_id=target(base - G + s, tp), device_id_type=pl.DeviceIdType.MESH,
                ).wait_recv()
                kvf[at] = kv[at].astype(F32)

    @pl.when(jnp.logical_not(has_prev))
    def _():
        kvf[:own0] = jnp.zeros((own0, BACK, LANES), F32)

    arrive(range(G - 4 // halves, G))
    run([tile1(0, 2)])
    run([tile4(0, r, 3) for r in range(4)])

    arrive(range(G - 4 // halves))

    @pl.loop(0, 4)
    def _(i):
        run([tile16(4 * i + n) for n in range(4)])

    @pl.loop(0, nq)
    def _(h):
        o = acc[h]
        y = o / pltpu.roll(o, HD, 1)
        rs[h] = jnp.where(low[: HD], pltpu.roll(y[:HD], HD, 1), y[HD:]).astype(BF16)

    def copy_ret(n):
        return pltpu.make_async_remote_copy(
            src_ref=rs.at[n], dst_ref=rr.at[head], send_sem=s_ret.at[n], recv_sem=r_ret.at[head],
            device_id=target(base + n // tp_count, lax.rem(n, tp_count)),
            device_id_type=pl.DeviceIdType.MESH,
        )

    for o in far + [0]:
        copy_ret(mate(o) * tp_count + tp_count - 1 - tp).start()
        if o:
            copy_ret(mate(o) * tp_count + tp).start()
    rr[head] = rs[seat]

    for o in range(1, G):
        copy_kv(lax.rem(me + o, G)).wait_send()
        copy_q(lax.rem(me + o, G)).wait_send()

    @pl.when(has_next)
    def _():
        for o in range(G):
            copy_x(lax.rem(me + o, G)).wait_send()

    w_local.wait()
    w_away.wait_send()
    pltpu.make_async_remote_copy(
        src_ref=w_ref, dst_ref=wbuf.at[tp_count - 1 - tp],
        send_sem=w_sem.at[1], recv_sem=w_sem.at[2],
        device_id=target(sp, tp_count - 1 - tp), device_id_type=pl.DeviceIdType.MESH,
    ).wait_recv()

    for o in range(1, seats):
        n = lax.rem(seat - o + seats, seats)
        their = lax.rem(n, tp_count) * G + n // tp_count
        pltpu.make_async_remote_copy(
            src_ref=rs.at[n], dst_ref=rr.at[their], send_sem=s_ret.at[n],
            recv_sem=r_ret.at[their],
            device_id=target(base + n // tp_count, lax.rem(n, tp_count)),
            device_id_type=pl.DeviceIdType.MESH,
        ).wait_recv()

    low_h = low[:HD]
    for m in range(seats // 2):
        x0 = rr[2 * m].astype(F32)
        x1 = rr[2 * m + 1].astype(F32)
        pair = jnp.concatenate(
            [jnp.where(low_h, x0, pltpu.roll(x1, HD, 1)), jnp.where(low_h, pltpu.roll(x0, HD, 1), x1)],
            axis=0,
        ).astype(BF16)
        mx[:, m * LANES : (m + 1) * LANES] = jnp.dot(
            back, pair, preferred_element_type=F32
        ).astype(BF16)

    width = wbuf.shape[1]
    step = 512

    @pl.loop(0, out_ref.shape[1] // step)
    def _(c):
        cols = pl.ds(pl.multiple_of(c * step, step), step)
        total = jnp.dot(mx[:, :width], wbuf[0, :, cols], preferred_element_type=F32)
        total = total + jnp.dot(mx[:, width:], wbuf[1, :, cols], preferred_element_type=F32)
        out_ref[:, cols] = total.astype(BF16)

    for o in range(1, seats):
        copy_ret(lax.rem(seat + o, seats)).wait_send()


def per_device(sp_count, tp_count, query_rows, key_rows, value_rows, out_weight):
    tok = query_rows.shape[0]
    G = query_rows.shape[1] // HD
    halves = tok // BACK
    ngroups = sp_count // G
    assert tok == 2 * BACK and tp_count == 2 and sp_count % G == 0
    assert G & (G - 1) == 0
    assert G * tok == 16 * BACK
    inverse = np.power(THETA, -np.arange(HD // 2) / (HD // 2))
    inverse = np.tile(inverse, LANES // (HD // 2))[None, :]
    local = np.arange(tok)[:, None] * inverse
    cosb = jnp.asarray(np.cos(local), F32)
    sinb = jnp.asarray(np.sin(local), F32)
    inv = jnp.asarray(np.tile(inverse, (8, 1)), F32)
    seats = G * tp_count
    vmem = pl.BlockSpec(memory_space=pltpu.VMEM)
    dma = pltpu.SemaphoreType.DMA
    return pl.pallas_call(
        functools.partial(kernel, G, ngroups, tp_count),
        out_shape=jax.ShapeDtypeStruct((tok // tp_count, out_weight.shape[1]), BF16),
        in_specs=[pl.BlockSpec(memory_space=pl.ANY)] * 7,
        out_specs=vmem,
        scratch_shapes=[
            pltpu.VMEM(query_rows.shape, BF16),
            pltpu.VMEM(query_rows.shape, BF16),
            pltpu.VMEM(query_rows.shape, BF16),
            pltpu.VMEM(cosb.shape, F32),
            pltpu.VMEM(sinb.shape, F32),
            pltpu.VMEM(inv.shape, F32),
            pltpu.VMEM((G, BACK, LANES), BF16),
            pltpu.VMEM((G, halves, BACK, LANES), BF16),
            pltpu.VMEM((G, BACK, LANES), BF16),
            pltpu.VMEM((2 * G * halves, BACK, LANES), BF16),
            pltpu.VMEM((2 * G * halves, BACK, LANES), F32),
            pltpu.VMEM((G * halves, BACK, LANES), BF16),
            pltpu.VMEM((G * halves, BACK, LANES), F32),
            pltpu.VMEM((G * halves, BACK, LANES), F32),
            pltpu.VMEM((G * halves, BACK, LANES), F32),
            pltpu.VMEM((5, BACK, 2 * BACK), F32),
            pltpu.VMEM((tp_count,) + out_weight.shape, BF16),
            pltpu.VMEM((seats, HD, LANES), BF16),
            pltpu.VMEM((seats, HD, LANES), BF16),
            pltpu.VMEM((BACK, seats * HD), BF16),
            dma((G,)), dma((G,)), dma((G,)), dma((G,)), dma((G,)), dma((G,)),
            dma((3,)), dma((seats,)), dma((seats,)), dma((6,)),
        ],
        compiler_params=pltpu.CompilerParams(
            collective_id=0, has_side_effects=True, vmem_limit_bytes=63 * 1024 * 1024
        ),
    )(query_rows, key_rows, value_rows, cosb, sinb, inv, out_weight)


def solution(mesh):
    return jax.shard_map(
        functools.partial(per_device, mesh.shape["sp"], mesh.shape["tp"]),
        mesh=mesh,
        in_specs=(P("sp", "tp"), P("sp", "tp"), P("sp", "tp"), P("tp", None)),
        out_specs=P(("sp", "tp"), None),
        check_vma=False,
    )
```

profile of v0, /device:TPU:17, one launch (start us, length us, event | category | flops | bytes accessed | tf_op | source)
XLA Modules:
  0.0 43.0 jit_solution(5179866640697724688)
XLA Ops:
  0.0 41.1 %shard_map.73 = bf16[128,2048]{1,0:T(8,128)(2,1)} custom-call(bf16[256,512]{1,0:T(8,128)(2,1)} %q_hbm.1, bf16[256,512]{1,0:T(8,128)(2,1)} %k_hbm.1, bf16[256,512]{1,0:T(8,128)(2,1)} %v_hbm.1, f32[256,128]{1,0:T(8,128)} %constant.6.clone.cosb_hbm, f32[256,128]{1,0:T(8,128)} %constant.7.clone.sinb_hbm, f32[8,128]{1,0:T(8,128)} %constant.8.clone.inv_hbm, ...), custom_call_target="tpu_custom_call" | custom-call | tf_op jit(solution)/shard_map/pallas_call | solution.py:404
  41.1 1.9 %copy.9 = bf16[128,2048]{1,0:T(8,128)(2,1)} copy(bf16[128,2048]{1,0:T(8,128)(2,1)} %shard_map.73) | data formatting | bytes 1048576
where the time goes:
time: 43.2 us; the launch traced here: 43 us
  Pallas kernels  41.1 us (95%)
  local copies, waits for them, and re-layouts  1.88 us (4%)
    pallas_call x1, Pallas kernels, per_device(): pl.pallas_call(functools.partial(kernel, G, ngroups, tp_count), out_shape...  41.1 us
    unnamed x1, local copies, waits for them, and re-layouts  1.88 us

commit v1 on v0

v1 whole, which is shorter than its diff:
```python
import functools
import math

import jax
import jax.numpy as jnp
import numpy as np
from jax import lax
from jax.experimental import pallas as pl
from jax.experimental.pallas import tpu as pltpu
from jax.sharding import PartitionSpec as P

HD = 64
BACK = 128
THETA = 500000.0
FAR = -1e30
F32 = jnp.float32
BF16 = jnp.bfloat16
LANES = 2 * HD
CHUNKS = 4
PIECE = BACK // CHUNKS
NT = (((1,), (1,)), ((), ()))


def place(p):
    return ((p & 7) << 4) + (((p >> 3) & 3) << 2) + (p >> 5)


def iota(shape, axis):
    return lax.broadcasted_iota(jnp.int32, shape, axis)


def kernel(
    G, ngroups, tp_count,
    q_hbm, k_hbm, v_hbm, cosb_hbm, sinb_hbm, inv_hbm, w_ref, out_ref,
    q_ref, k_ref, v_ref, cosb_ref, sinb_ref, inv_ref, qs, kvs, qr, kv, kvf, q2, q2f, acc, top,
    qb, qbf, accb, topb, ob, oin, b1_ref, b4_ref, b16_ref, wbuf, rs, rr, mx,
    s_kv, s_q, s_qb, s_x, s_o, s_ret, r_kv, r_q, r_qb, r_x, r_o, r_ret, w_sem, in_sem,
):
    loads = [
        pltpu.make_async_copy(source, dest, in_sem.at[n])
        for n, (source, dest) in enumerate((
            (inv_hbm, inv_ref), (cosb_hbm, cosb_ref), (sinb_hbm, sinb_ref),
            (k_hbm, k_ref), (v_hbm, v_ref), (q_hbm, q_ref),
        ))
    ]
    for load in loads:
        load.start()
    sp = lax.axis_index("sp")
    tp = lax.axis_index("tp")
    group = sp // G
    me = sp - group * G
    base = group * G
    has_prev = group > 0
    has_next = group < ngroups - 1
    seat = me * tp_count + tp
    seats = G * tp_count
    head = tp * G + me
    tok = q_ref.shape[0]
    halves = tok // BACK
    nq = G * halves
    own0 = 1

    def target(s, t):
        return {"sp": s, "tp": t}

    barrier = pltpu.get_barrier_semaphore()
    for o in range(1, seats):
        n = lax.rem(seat + o, seats)
        pl.semaphore_signal(
            barrier, inc=1, device_id=target(base + n // tp_count, lax.rem(n, tp_count)),
            device_id_type=pl.DeviceIdType.MESH,
        )

    @pl.when(has_prev)
    def _():
        for o in range(G):
            pl.semaphore_signal(
                barrier, inc=1, device_id=target(base - G + o, tp),
                device_id_type=pl.DeviceIdType.MESH,
            )

    @pl.when(has_next)
    def _():
        for o in range(G):
            pl.semaphore_signal(
                barrier, inc=1, device_id=target(base + G + o, tp),
                device_id_type=pl.DeviceIdType.MESH,
            )

    w_local = pltpu.make_async_copy(w_ref, wbuf.at[tp], w_sem.at[0])
    w_local.start()

    def stride4(n):
        w = n & 31
        return ((n >> 5) << 5) + ((w & 7) << 2) + (w >> 3)

    def masked(distance):
        return jnp.where((distance >= 0) & (distance <= BACK), 0.0, FAR)

    row = iota((BACK, 2 * BACK), 0)
    col = iota((BACK, 2 * BACK), 1)
    b1_ref[...] = masked(place(row) + BACK - place(col & (BACK - 1)) - ((col >> 7) << 7))
    b4_ref[...] = masked(stride4(row) + BACK - stride4(col))
    b16_ref[...] = masked(row + BACK - col)

    scope = jax.named_scope
    with scope("a_loads"):
        for load in loads:
            load.wait()

    lane = iota((BACK, LANES), 1)
    low = lane < HD
    lane_t = iota((tok, LANES), 1)
    first = (lane_t & (HD - 1)) < HD // 2
    angle = inv_ref[...] * (sp * tok).astype(F32)
    ca = jnp.cos(angle)[:1]
    sa = jnp.sin(angle)[:1]
    cos = ca * cosb_ref[...] - sa * sinb_ref[...]
    sin = sa * cosb_ref[...] + ca * sinb_ref[...]
    sin = jnp.where(first, -sin, sin)
    swizzle = jnp.where(place(iota((BACK, BACK), 0)) == iota((BACK, BACK), 1), 1.0, 0.0).astype(BF16)
    back = jnp.where(place(iota((BACK, BACK), 1)) == iota((BACK, BACK), 0), 1.0, 0.0).astype(BF16)

    def turn(ref, cols):
        x = ref[:, cols].astype(F32)
        other = jnp.where(first, pltpu.roll(x, LANES - HD // 2, 1), pltpu.roll(x, HD // 2, 1))
        return (x * cos + other * sin).astype(BF16)

    def sw(x):
        return jnp.dot(swizzle, x, preferred_element_type=F32)

    def cut(x):
        return x.astype(BF16).reshape(CHUNKS, PIECE, LANES)

    with scope("c_turn"):
        for m in range(G // 2):
            cols = slice(m * LANES, (m + 1) * LANES)
            tq = turn(q_ref, cols)
            tk = turn(k_ref, cols)
            tv = v_ref[:, cols]
            q_a = sw(tq[:BACK]) * (1.0 / math.sqrt(HD))
            q_b = sw(tq[BACK:]) * (1.0 / math.sqrt(HD))
            qs[:, 2 * m] = cut(jnp.where(low, q_a, pltpu.roll(q_b, HD, 1)))
            qs[:, 2 * m + 1] = cut(jnp.where(low, pltpu.roll(q_a, HD, 1), q_b))
            for e in range(halves):
                ks = sw(tk[e * BACK : (e + 1) * BACK])
                vs = sw(tv[e * BACK : (e + 1) * BACK])
                kvs[:, 2 * m, e] = cut(jnp.where(low, ks, pltpu.roll(vs, HD, 1)))
                kvs[:, 2 * m + 1, e] = cut(jnp.where(low, pltpu.roll(ks, HD, 1), vs))

    with scope("d_barrier"):
        pl.semaphore_wait(
            barrier, seats - 1 + jnp.where(has_prev, G, 0) + jnp.where(has_next, G, 0)
        )

    def remote(source, dest, send, recv, device):
        return pltpu.make_async_remote_copy(
            src_ref=source, dst_ref=dest, send_sem=send, recv_sem=recv,
            device_id=device, device_id_type=pl.DeviceIdType.MESH,
        )

    def drain(ref, sem):
        pltpu.make_async_copy(ref, ref, sem).wait()

    def copy_kv(c, dest):
        return remote(
            kvs.at[c, dest], kv.at[c, pl.ds(own0 + halves * me, halves)],
            s_kv, r_kv.at[c], target(base + dest, tp),
        )

    def copy_q(c, dest):
        return remote(qs.at[c, dest], qr.at[c, me], s_q, r_q.at[c], target(base + dest, tp))

    def copy_qb(c, dest):
        return remote(
            qs.at[c, dest], qb.at[c, me], s_qb, r_qb.at[c], target(base - G + dest, tp)
        )

    w_away = pltpu.make_async_remote_copy(
        src_ref=w_ref, dst_ref=wbuf.at[tp], send_sem=w_sem.at[1], recv_sem=w_sem.at[2],
        device_id=target(sp, tp_count - 1 - tp), device_id_type=pl.DeviceIdType.MESH,
    )

    bits = [1 << n for n in range(G.bit_length() - 1)]
    far = sorted(range(1, G), key=lambda o: -o.bit_count())

    def mate(o):
        return sum((((me // b + o // b) % 2) * b for b in bits), 0)

    with scope("e_issue"):
        for c in range(CHUNKS):
            @pl.when(has_prev)
            def _():
                for o in [*far, 0]:
                    copy_qb(c, mate(o)).start()

            for o in far:
                copy_q(c, mate(o)).start()
                copy_kv(c, mate(o)).start()

        w_away.start()

    for c in range(CHUNKS):
        kv[c, pl.ds(own0 + halves * me, halves)] = kvs[c, me]
        qr[c, me] = qs[c, me]

    low_p = low[:PIECE]

    def unpack(ref, c, wide, narrow=None):
        for s in range(G):
            x = ref[c, s].astype(F32)
            a = jnp.where(low_p, x, 0.0)
            b = jnp.where(low_p, pltpu.roll(x, HD, 1), 0.0)
            wide[2 * s] = a
            wide[2 * s + 1] = b
            if narrow is not None:
                narrow[c, 2 * s] = a.astype(BF16)
                narrow[c, 2 * s + 1] = b.astype(BF16)

    def run(tiles, fresh=False, sums=acc, tops=top):
        done = []
        for q, keys, b, ref_at in tiles:
            s = lax.dot_general(q, keys, NT, preferred_element_type=F32) + b
            t = jnp.max(s, axis=1, keepdims=True)
            shape = sums[ref_at].shape
            if fresh:
                t = jnp.broadcast_to(t, (q.shape[0], LANES))
            else:
                t_old = tops[ref_at].reshape(-1, LANES)
                t = jnp.maximum(t_old, t)
            p = jnp.concatenate(
                [jnp.exp(s[:, n : n + LANES] - t) for n in range(0, s.shape[1], LANES)], axis=1
            ).astype(BF16)
            ones = jnp.where(iota(keys.shape, 1) < HD, jnp.ones_like(keys), keys)
            o = jnp.dot(p, ones, preferred_element_type=F32)
            if not fresh:
                o = sums[ref_at].reshape(-1, LANES) * jnp.exp(t_old - t) + o
            done.append((ref_at, o.reshape(shape), t.reshape(shape)))
        for ref_at, o, t in done:
            sums[ref_at] = o
            tops[ref_at] = t

    every = slice(None)

    def block(h):
        return kv[:, own0 + h].reshape(BACK, LANES)

    def tile1(h):
        return (
            q2[:, h].reshape(BACK, LANES), jnp.concatenate([block(h - 1), block(h)], axis=0),
            b1_ref[...], (every, h),
        )

    def tile1_part(e):
        return (
            q2[:, 0].reshape(BACK, LANES), block(e - 1),
            b1_ref[:, e * BACK : (e + 1) * BACK], (every, 0),
        )

    def tile4(c, n):
        blocks = slice(4 * n, 4 * n + 4)
        return (
            q2[c, blocks].reshape(BACK, LANES),
            kv[c, own0 + 4 * n - 4 : own0 + 4 * n + 4].reshape(2 * BACK, LANES),
            b4_ref[...], (c, blocks),
        )

    def tile4_new(c):
        return (
            q2[c, :4].reshape(BACK, LANES), kv[c, own0 : own0 + 4].reshape(BACK, LANES),
            b4_ref[:, BACK:], (c, slice(0, 4)),
        )

    def tile4_old(c):
        return (
            qbf[:4].reshape(BACK, LANES).astype(BF16),
            kv[c, own0 + nq - 4 : own0 + nq].reshape(BACK, LANES),
            b4_ref[:, :BACK], (slice(0, 4),),
        )

    def tile16(i, queries, e, ref_at):
        rows = slice(8 * i, 8 * i + 8)
        return (
            queries[:, rows].reshape(BACK, LANES).astype(BF16),
            kvf[:, rows].reshape(BACK, LANES).astype(BF16),
            b16_ref[:, e * BACK : (e + 1) * BACK], (*ref_at, every, rows),
        )

    each = range(PIECE // 8)
    half = PIECE // 2
    eight = BACK // half
    lane_h = iota((eight, half, LANES), 2)
    low_h = lane_h < HD
    flat = (BACK, LANES)

    def rounded(x):
        return x.astype(BF16).astype(F32)

    def send_old(c):
        stats = jnp.zeros((2 * 8, LANES), F32)
        for g in range(nq // eight):
            at = slice(g * eight, (g + 1) * eight)
            t = topb[at]
            mark = rounded(t)
            a = accb[at] * jnp.exp(t - mark)
            z = pltpu.roll(a, HD, 2)
            lo, hi = a[:, :half], a[:, half:]
            ob[c, g * BACK : (g + 1) * BACK] = (
                jnp.where(low_h, z[:, :half], hi).astype(BF16).reshape(flat)
            )
            columns = mark[:, half:]
            columns = jnp.where(lane_h == 0, mark[:, :half], columns)
            columns = jnp.where(lane_h == 2, rounded(lo), columns)
            columns = jnp.where(lane_h == 3, rounded(hi), columns)
            columns = jnp.where(lane_h == 4, lo - rounded(lo), columns)
            columns = jnp.where(lane_h == 5, hi - rounded(hi), columns)
            pick = (iota((2 * 8, LANES), 0) - 8 * g == iota((2 * 8, LANES), 1)) & (
                iota((2 * 8, LANES), 1) < 6
            )
            stats = stats + lax.dot_general(
                jnp.where(pick, 1.0, 0.0).astype(BF16), columns.astype(BF16).reshape(flat), NT,
                preferred_element_type=F32,
            )
        ob[c, nq * half :] = stats.astype(BF16)
        copy_o(c).start()

    def copy_o(c):
        return remote(ob.at[c], oin.at[c], s_o, r_o.at[c], target(sp + G, tp))

    def copy_x():
        return remote(kv.at[:, own0 + nq - 1], kv.at[:, 0], s_x, r_x, target(sp + G, tp))

    with scope("h_chunks"):
        @pl.loop(0, CHUNKS)
        def _(c):
            drain(qr.at[c, : G - 1], r_q.at[c])
            drain(kv.at[c, own0 : own0 + halves * (G - 1)], r_kv.at[c])
            kvf[...] = kv[c, own0:].astype(F32)

            @pl.when(has_next)
            def _():
                drain(qb.at[c], r_qb.at[c])
                unpack(qb, c, qbf)
                run([tile16(i, qbf, 0, ()) for i in each], True, accb, topb)
                run([tile4_old(c)], False, accb, topb)
                send_old(c)

            unpack(qr, c, q2f, q2)
            run([tile4_new(c)] + [tile4(c, n) for n in range(1, nq // 4)], True)
            run([tile16(i, q2f, 1, (c,)) for i in each])

    with scope("i_t1"):
        @pl.when(has_next)
        def _():
            copy_x().start()

        run([tile1_part(1)])

        @pl.loop(0, (nq - 1) // 5)
        def _(i):
            run([tile1(1 + 5 * i + n) for n in range(5)])

        @pl.when(has_prev)
        def _():
            drain(kv.at[:, 0], r_x)
            run([tile1_part(0)])

    eye = jnp.where(iota(flat, 0) == iota(flat, 1), 1.0, 0.0).astype(BF16)
    upper = iota(flat, 0) < HD

    def finish(c, merge):
        if merge:
            stats = oin[c, nq * half :].astype(F32)
        for g in range(nq // eight):
            at = slice(g * eight, (g + 1) * eight)
            a = acc[c, at]
            z = pltpu.roll(a, HD, 2)
            num = jnp.where(low_h, z[:, :half], a[:, half:]).reshape(flat)
            den = jnp.where(low_h, a[:, :half], z[:, half:]).reshape(flat)
            if merge:
                def spread(j):
                    both = jnp.where(
                        upper,
                        jnp.broadcast_to(stats[8 * g + j : 8 * g + j + 1], flat),
                        jnp.broadcast_to(stats[8 * g + j + 1 : 8 * g + j + 2], flat),
                    )
                    return lax.dot_general(eye, both.astype(BF16), NT, preferred_element_type=F32)

                t = top[c, at]
                t = jnp.where(low_h, t[:, :half], t[:, half:]).reshape(flat)
                t_old = spread(0)
                t_new = jnp.maximum(t, t_old)
                mine = jnp.exp(t - t_new)
                theirs = jnp.exp(t_old - t_new)
                num = num * mine + oin[c, g * BACK : (g + 1) * BACK].astype(F32) * theirs
                den = den * mine + (spread(2) + spread(4)) * theirs
            rs[c, at] = (num / den).astype(BF16).reshape(eight, half, LANES)

    def copy_ret(c, n):
        return remote(
            rs.at[c, n], rr.at[c, head], s_ret, r_ret,
            target(base + n // tp_count, lax.rem(n, tp_count)),
        )

    with scope("o_finish"):
        @pl.loop(0, CHUNKS)
        def _(c):
            @pl.when(has_prev)
            def _():
                drain(oin.at[c], r_o.at[c])
                finish(c, True)

            @pl.when(jnp.logical_not(has_prev))
            def _():
                finish(c, False)

            for o in far + [0]:
                copy_ret(c, mate(o) * tp_count + tp_count - 1 - tp).start()
                if o:
                    copy_ret(c, mate(o) * tp_count + tp).start()
            rr[c, head] = rs[c, seat]

    with scope("q_sendwait"):
        drain(kvs.at[:, : G - 1], s_kv)
        drain(qs.at[:, : G - 1], s_q)

        @pl.when(has_prev)
        def _():
            drain(qs, s_qb)

        @pl.when(has_next)
        def _():
            drain(ob, s_o)
            drain(kv.at[:, 0], s_x)

        w_local.wait()
        w_away.wait_send()
        pltpu.make_async_remote_copy(
            src_ref=w_ref, dst_ref=wbuf.at[tp_count - 1 - tp],
            send_sem=w_sem.at[1], recv_sem=w_sem.at[2],
            device_id=target(sp, tp_count - 1 - tp), device_id_type=pl.DeviceIdType.MESH,
        ).wait_recv()

    with scope("s_retwait"):
        drain(rr.at[:, : seats - 1], r_ret)

    low_s = iota((half, LANES), 1) < HD
    with scope("t_mix"):
        for m in range(seats // 2):
            x0 = rr[:, 2 * m].astype(F32)
            x1 = rr[:, 2 * m + 1].astype(F32)
            y0 = pltpu.roll(x0, HD, 2)
            y1 = pltpu.roll(x1, HD, 2)
            pair = jnp.concatenate(
                [jnp.where(low_s[None], x0, y1), jnp.where(low_s[None], y0, x1)], axis=1
            ).astype(BF16).reshape(BACK, LANES)
            mx[:, m * LANES : (m + 1) * LANES] = jnp.dot(
                back, pair, preferred_element_type=F32
            ).astype(BF16)

    width = wbuf.shape[1]
    step = 512

    with scope("u_proj"):
        @pl.loop(0, out_ref.shape[1] // step)
        def _(c):
            cols = pl.ds(pl.multiple_of(c * step, step), step)
            total = jnp.dot(mx[:, :width], wbuf[0, :, cols], preferred_element_type=F32)
            total = total + jnp.dot(mx[:, width:], wbuf[1, :, cols], preferred_element_type=F32)
            out_ref[:, cols] = total.astype(BF16)

    with scope("v_end"):
        drain(rs.at[:, : seats - 1], s_ret)


def per_device(sp_count, tp_count, query_rows, key_rows, value_rows, out_weight):
    tok = query_rows.shape[0]
    G = query_rows.shape[1] // HD
    halves = tok // BACK
    ngroups = sp_count // G
    assert tok == 2 * BACK and tp_count == 2 and sp_count % G == 0
    assert G & (G - 1) == 0
    assert G * tok == 16 * BACK
    inverse = np.power(THETA, -np.arange(HD // 2) / (HD // 2))
    inverse = np.tile(inverse, LANES // (HD // 2))[None, :]
    local = np.arange(tok)[:, None] * inverse
    cosb = jnp.asarray(np.cos(local), F32)
    sinb = jnp.asarray(np.sin(local), F32)
    inv = jnp.asarray(np.tile(inverse, (8, 1)), F32)
    seats = G * tp_count
    nq = G * halves
    vmem = pl.BlockSpec(memory_space=pltpu.VMEM)
    dma = pltpu.SemaphoreType.DMA
    return pl.pallas_call(
        functools.partial(kernel, G, ngroups, tp_count),
        out_shape=pltpu.VMEM((tok // tp_count, out_weight.shape[1]), BF16),
        in_specs=[pl.BlockSpec(memory_space=pl.ANY)] * 7,
        out_specs=vmem,
        scratch_shapes=[
            pltpu.VMEM(query_rows.shape, BF16),
            pltpu.VMEM(query_rows.shape, BF16),
            pltpu.VMEM(query_rows.shape, BF16),
            pltpu.VMEM(cosb.shape, F32),
            pltpu.VMEM(sinb.shape, F32),
            pltpu.VMEM(inv.shape, F32),
            pltpu.VMEM((CHUNKS, G, PIECE, LANES), BF16),
            pltpu.VMEM((CHUNKS, G, halves, PIECE, LANES), BF16),
            pltpu.VMEM((CHUNKS, G, PIECE, LANES), BF16),
            pltpu.VMEM((CHUNKS, 1 + nq, PIECE, LANES), BF16),
            pltpu.VMEM((nq, PIECE, LANES), F32),
            pltpu.VMEM((CHUNKS, nq, PIECE, LANES), BF16),
            pltpu.VMEM((nq, PIECE, LANES), F32),
            pltpu.VMEM((CHUNKS, nq, PIECE, LANES), F32),
            pltpu.VMEM((CHUNKS, nq, PIECE, LANES), F32),
            pltpu.VMEM((CHUNKS, G, PIECE, LANES), BF16),
            pltpu.VMEM((nq, PIECE, LANES), F32),
            pltpu.VMEM((nq, PIECE, LANES), F32),
            pltpu.VMEM((nq, PIECE, LANES), F32),
            pltpu.VMEM((CHUNKS, nq * PIECE // 2 + 16, LANES), BF16),
            pltpu.VMEM((CHUNKS, nq * PIECE // 2 + 16, LANES), BF16),
            pltpu.VMEM((BACK, 2 * BACK), F32),
            pltpu.VMEM((BACK, 2 * BACK), F32),
            pltpu.VMEM((BACK, 2 * BACK), F32),
            pltpu.VMEM((tp_count,) + out_weight.shape, BF16),
            pltpu.VMEM((CHUNKS, seats, PIECE // 2, LANES), BF16),
            pltpu.VMEM((CHUNKS, seats, PIECE // 2, LANES), BF16),
            pltpu.VMEM((BACK, seats * HD), BF16),
            dma, dma, dma, dma, dma, dma,
            dma((CHUNKS,)), dma((CHUNKS,)), dma((CHUNKS,)), dma, dma((CHUNKS,)), dma,
            dma((3,)), dma((6,)),
        ],
        compiler_params=pltpu.CompilerParams(
            collective_id=0, has_side_effects=True, vmem_limit_bytes=63 * 1024 * 1024
        ),
    )(query_rows, key_rows, value_rows, cosb, sinb, inv, out_weight)


def solution(mesh):
    return jax.shard_map(
        functools.partial(per_device, mesh.shape["sp"], mesh.shape["tp"]),
        mesh=mesh,
        in_specs=(P("sp", "tp"), P("sp", "tp"), P("sp", "tp"), P("tp", None)),
        out_specs=P(("sp", "tp"), None),
        check_vma=False,
    )
```

time: 43.2 us -> 35.7 us (0.83)
  Pallas kernels: 41.1 us -> 34.4 us
  local copies, waits for them, and re-layouts: 1.88 us -> 0.8 us
    pallas_call x1, Pallas kernels: 41.1 us -> 34.4 us  [per_device(): pl.pallas_call(functools.partial(kernel, G, ngroups, tp_count), out_shape...]
    unnamed x1, local copies, waits for them, and re-layouts: 1.88 us -> 0.8 us
where the time goes in v1:
time: 35.7 us; the launch traced here: 35.2 us
  Pallas kernels  34.4 us (96%)
  local copies, waits for them, and re-layouts  0.8 us (2%)
    pallas_call x1, Pallas kernels, per_device(): pl.pallas_call(functools.partial(kernel, G, ngroups, tp_count), out_shape...  34.4 us
    unnamed x1, local copies, waits for them, and re-layouts  0.8 us

profile of v1, /device:TPU:17, one launch (start us, length us, event | category | flops | bytes accessed | tf_op | source)
XLA Modules:
  0.0 35.2 jit_solution(1361160453988191689)
XLA Ops:
  0.0 34.4 %shard_map.73 = bf16[128,2048]{1,0:T(8,128)(2,1)S(1)} custom-call(bf16[256,512]{1,0:T(8,128)(2,1)} %q_hbm.1, bf16[256,512]{1,0:T(8,128)(2,1)} %k_hbm.1, bf16[256,512]{1,0:T(8,128)(2,1)} %v_hbm.1, f32[256,128]{1,0:T(8,128)} %constant.6.clone.cosb_hbm, f32[256,128]{1,0:T(8,128)} %constant.7.clone.sinb_hbm, f32[8,128]{1,0:T(8,128)} %constant.8.clone.inv_hbm, ...), custom_call_target="tpu_custom_call" | custom-call | tf_op jit(solution)/shard_map/pallas_call | solution.py:494
  34.4 0.8 %copy.9 = bf16[128,2048]{1,0:T(8,128)(2,1)} copy(bf16[128,2048]{1,0:T(8,128)(2,1)S(1)} %shard_map.73) | data formatting | bytes 1048576

commit v2 on v1

--- a/solution.py
+++ b/solution.py
@@ -32,8 +32,8 @@
 def kernel(
     G, ngroups, tp_count,
     q_hbm, k_hbm, v_hbm, cosb_hbm, sinb_hbm, inv_hbm, w_ref, out_ref,
-    q_ref, k_ref, v_ref, cosb_ref, sinb_ref, inv_ref, qs, kvs, qr, kv, kvf, q2, q2f, acc, top,
-    qb, qbf, accb, topb, ob, oin, b1_ref, b4_ref, b16_ref, wbuf, rs, rr, mx,
+    q_ref, k_ref, v_ref, cosb_ref, sinb_ref, inv_ref, qs, kvs, qr, kv, kvf, q2, q2f,
+    acc1, top1, acc4, top4, acc16, top16, accx, topx, qb, qbf, accb, topb, accb4, topb4, ob, oin, pn, pd, pt, b1_ref, b4_ref, b16_ref, bx_ref, wbuf, rs, rr, mx,
     s_kv, s_q, s_qb, s_x, s_o, s_ret, r_kv, r_q, r_qb, r_x, r_o, r_ret, w_sem, in_sem,
 ):
     loads = [
@@ -58,7 +58,9 @@
     tok = q_ref.shape[0]
     halves = tok // BACK
     nq = G * halves
-    own0 = 1
+    hb = G // 2
+    nh = nq // 2
+    own0 = nh
 
     def target(s, t):
         return {"sp": s, "tp": t}
@@ -102,6 +104,14 @@
     b1_ref[...] = masked(place(row) + BACK - place(col & (BACK - 1)) - ((col >> 7) << 7))
     b4_ref[...] = masked(stride4(row) + BACK - stride4(col))
     b16_ref[...] = masked(row + BACK - col)
+
+    def stride16(n):
+        return ((n >> 4) << 3) + (n & 7)
+
+    xrow = iota((BACK, BACK), 0)
+    xcol = iota((BACK, BACK), 1)
+    same = ((xrow ^ xcol) & 8) == 0
+    bx_ref[...] = jnp.where(same, masked(stride16(xrow) + BACK - stride16(xcol)), FAR)
 
     scope = jax.named_scope
     with scope("a_loads"):
@@ -176,6 +186,12 @@
             qs.at[c, dest], qb.at[c, me], s_qb, r_qb.at[c], target(base - G + dest, tp)
         )
 
+    def copy_x(c, dest):
+        return remote(
+            kvs.at[c, dest], kv.at[c, pl.ds(halves * (me - hb), halves)],
+            s_x, r_x, target(base + G + dest, tp),
+        )
+
     w_away = pltpu.make_async_remote_copy(
         src_ref=w_ref, dst_ref=wbuf.at[tp], send_sem=w_sem.at[1], recv_sem=w_sem.at[2],
         device_id=target(sp, tp_count - 1 - tp), device_id_type=pl.DeviceIdType.MESH,
@@ -184,12 +200,21 @@
     bits = [1 << n for n in range(G.bit_length() - 1)]
     far = sorted(range(1, G), key=lambda o: -o.bit_count())
 
+    quad = [o for o in far if o < hb] + [0]
+
     def mate(o):
         return sum((((me // b + o // b) % 2) * b for b in bits), 0)
 
     with scope("e_issue"):
+        @pl.when(jnp.logical_and(has_next, me >= hb))
+        def _():
+            for part in (0, hb):
+                for c in range(CHUNKS):
+                    for o in quad:
+                        copy_x(c, part + lax.rem(mate(o), hb)).start()
+
         for c in range(CHUNKS):
-            @pl.when(has_prev)
+            @pl.when(jnp.logical_and(has_prev, me < hb))
             def _():
                 for o in [*far, 0]:
                     copy_qb(c, mate(o)).start()
@@ -198,8 +223,6 @@
                 copy_q(c, mate(o)).start()
                 copy_kv(c, mate(o)).start()
 
-        w_away.start()
-
     for c in range(CHUNKS):
         kv[c, pl.ds(own0 + halves * me, halves)] = kvs[c, me]
         qr[c, me] = qs[c, me]
@@ -207,7 +230,7 @@
     low_p = low[:PIECE]
 
     def unpack(ref, c, wide, narrow=None):
-        for s in range(G):
+        for s in range(ref.shape[1]):
             x = ref[c, s].astype(F32)
             a = jnp.where(low_p, x, 0.0)
             b = jnp.where(low_p, pltpu.roll(x, HD, 1), 0.0)
@@ -217,28 +240,43 @@
                 narrow[c, 2 * s] = a.astype(BF16)
                 narrow[c, 2 * s + 1] = b.astype(BF16)
 
-    def run(tiles, fresh=False, sums=acc, tops=top):
+    def run(tiles):
         done = []
-        for q, keys, b, ref_at in tiles:
-            s = lax.dot_general(q, keys, NT, preferred_element_type=F32) + b
-            t = jnp.max(s, axis=1, keepdims=True)
-            shape = sums[ref_at].shape
-            if fresh:
-                t = jnp.broadcast_to(t, (q.shape[0], LANES))
-            else:
-                t_old = tops[ref_at].reshape(-1, LANES)
-                t = jnp.maximum(t_old, t)
-            p = jnp.concatenate(
-                [jnp.exp(s[:, n : n + LANES] - t) for n in range(0, s.shape[1], LANES)], axis=1
-            ).astype(BF16)
+        for tile in tiles:
+            q = jnp.concatenate([part[0] for part in tile], axis=0)
+            keys = jnp.concatenate([part[1] for part in tile], axis=0)
+            s = lax.dot_general(q, keys, NT, preferred_element_type=F32)
+            rows, cols, ps, ts = 0, 0, [], []
+            for part in tile:
+                n, k = part[0].shape[0], part[1].shape[0]
+                mine = s[rows : rows + n, cols : cols + k] + part[2]
+                t = jnp.max(mine, axis=1, keepdims=True)
+                p = [
+                    jnp.exp(mine[:, a : a + LANES] - t).astype(BF16) for a in range(0, k, LANES)
+                ]
+                none = jnp.zeros_like(p[0])
+                before, after = cols // LANES, (keys.shape[0] - cols - k) // LANES
+                ps.append(jnp.concatenate([none] * before + p + [none] * after, axis=1))
+                ts.append(t)
+                rows, cols = rows + n, cols + k
             ones = jnp.where(iota(keys.shape, 1) < HD, jnp.ones_like(keys), keys)
-            o = jnp.dot(p, ones, preferred_element_type=F32)
-            if not fresh:
-                o = sums[ref_at].reshape(-1, LANES) * jnp.exp(t_old - t) + o
-            done.append((ref_at, o.reshape(shape), t.reshape(shape)))
-        for ref_at, o, t in done:
-            sums[ref_at] = o
-            tops[ref_at] = t
+            o = jnp.dot(jnp.concatenate(ps, axis=0), ones, preferred_element_type=F32)
+            rows = 0
+            for part, t in zip(tile, ts):
+                end = rows + part[0].shape[0]
+                done.append((part[3], o[rows:end], jnp.broadcast_to(t, (end - rows, LANES))))
+                rows = end
+        for places, o, t in done:
+            first_row = 0
+            for sums, tops, at in places:
+                shape = sums[at].shape
+                rows = slice(first_row, first_row + math.prod(shape[:-1]))
+                sums[at] = o[rows].reshape(shape)
+                tops[at] = t[rows].reshape(shape)
+                first_row = rows.stop
+
+    def pairs(tiles):
+        return [tiles[n : n + 2] for n in range(0, len(tiles), 2)]
 
     every = slice(None)
 
@@ -248,13 +286,8 @@
     def tile1(h):
         return (
             q2[:, h].reshape(BACK, LANES), jnp.concatenate([block(h - 1), block(h)], axis=0),
-            b1_ref[...], (every, h),
-        )
-
-    def tile1_part(e):
-        return (
-            q2[:, 0].reshape(BACK, LANES), block(e - 1),
-            b1_ref[:, e * BACK : (e + 1) * BACK], (every, 0),
+            jnp.where(missing, FAR, b1_ref[...]) if h == 0 else b1_ref[...],
+            ((acc1, top1, (every, h)),),
         )
 
     def tile4(c, n):
@@ -262,28 +295,41 @@
         return (
             q2[c, blocks].reshape(BACK, LANES),
             kv[c, own0 + 4 * n - 4 : own0 + 4 * n + 4].reshape(2 * BACK, LANES),
-            b4_ref[...], (c, blocks),
-        )
-
-    def tile4_new(c):
-        return (
-            q2[c, :4].reshape(BACK, LANES), kv[c, own0 : own0 + 4].reshape(BACK, LANES),
-            b4_ref[:, BACK:], (c, slice(0, 4)),
-        )
+            b4_ref[...], ((acc4, top4, (c, blocks)),),
+        )
+
+    def tile4_first(c, alone):
+        keys = kv[c, own0 : own0 + 4].reshape(BACK, LANES)
+        b = b4_ref[:, BACK:]
+        if alone:
+            keys = jnp.concatenate([keys, keys], axis=0)
+            b = jnp.concatenate([jnp.full_like(b, FAR), b], axis=1)
+        return (q2[c, :4].reshape(BACK, LANES), keys, b, ((acc4, top4, (c, slice(0, 4))),))
 
     def tile4_old(c):
         return (
             qbf[:4].reshape(BACK, LANES).astype(BF16),
             kv[c, own0 + nq - 4 : own0 + nq].reshape(BACK, LANES),
-            b4_ref[:, :BACK], (slice(0, 4),),
-        )
-
-    def tile16(i, queries, e, ref_at):
+            b4_ref[:, :BACK], ((accb4, topb4, (every,)),),
+        )
+
+    def tile16(c, i, both):
         rows = slice(8 * i, 8 * i + 8)
+        q = q2f[c, :, rows].reshape(BACK, LANES).astype(BF16)
+        b = b16_ref[:, BACK:]
+        places = ((acc16, top16, (c, every, rows)),)
+        if both:
+            old = qbf[:, rows].reshape(-1, LANES).astype(BF16)
+            q = jnp.concatenate([q, old], axis=0)
+            b = jnp.concatenate([b, b16_ref[: old.shape[0], :BACK]], axis=0)
+            places = (*places, (accb, topb, (every, rows)))
+        return (q, kvf[:, rows].reshape(BACK, LANES).astype(BF16), b, places)
+
+    def tilex(c, i):
+        rows = slice(16 * i, 16 * i + 16)
         return (
-            queries[:, rows].reshape(BACK, LANES).astype(BF16),
-            kvf[:, rows].reshape(BACK, LANES).astype(BF16),
-            b16_ref[:, e * BACK : (e + 1) * BACK], (*ref_at, every, rows),
+            q2[c, nh:, rows].reshape(BACK, LANES), kv[c, :nh, rows].reshape(BACK, LANES),
+            bx_ref[...], ((accx, topx, (c, every, rows)),),
         )
 
     each = range(PIECE // 8)
@@ -297,8 +343,12 @@
         return x.astype(BF16).astype(F32)
 
     def send_old(c):
+        t4, t16 = topb4[...], topb[:4]
+        t = jnp.maximum(t4, t16)
+        accb[:4] = accb[:4] * jnp.exp(t16 - t) + accb4[...] * jnp.exp(t4 - t)
+        topb[:4] = t
         stats = jnp.zeros((2 * 8, LANES), F32)
-        for g in range(nq // eight):
+        for g in range(1):
             at = slice(g * eight, (g + 1) * eight)
             t = topb[at]
             mark = rounded(t)
@@ -321,14 +371,17 @@
                 jnp.where(pick, 1.0, 0.0).astype(BF16), columns.astype(BF16).reshape(flat), NT,
                 preferred_element_type=F32,
             )
-        ob[c, nq * half :] = stats.astype(BF16)
+        ob[c, BACK:] = stats.astype(BF16)
         copy_o(c).start()
 
     def copy_o(c):
         return remote(ob.at[c], oin.at[c], s_o, r_o.at[c], target(sp + G, tp))
 
-    def copy_x():
-        return remote(kv.at[:, own0 + nq - 1], kv.at[:, 0], s_x, r_x, target(sp + G, tp))
+    missing = jnp.logical_and(col < BACK, group == 0)
+
+    @pl.when(jnp.logical_not(has_prev))
+    def _():
+        kv[:, own0 - 1] = jnp.zeros((CHUNKS, PIECE, LANES), BF16)
 
     with scope("h_chunks"):
         @pl.loop(0, CHUNKS)
@@ -341,60 +394,81 @@
             def _():
                 drain(qb.at[c], r_qb.at[c])
                 unpack(qb, c, qbf)
-                run([tile16(i, qbf, 0, ()) for i in each], True, accb, topb)
-                run([tile4_old(c)], False, accb, topb)
+                unpack(qr, c, q2f.at[c], q2)
+                run(
+                    [*pairs([tile16(c, i, True) for i in each]), [tile4_old(c), tile4_first(c, False)]]
+                    + [[tile4(c, n)] for n in range(1, nq // 4)]
+                )
                 send_old(c)
 
-            unpack(qr, c, q2f, q2)
-            run([tile4_new(c)] + [tile4(c, n) for n in range(1, nq // 4)], True)
-            run([tile16(i, q2f, 1, (c,)) for i in each])
+            @pl.when(jnp.logical_not(has_next))
+            def _():
+                unpack(qr, c, q2f.at[c], q2)
+                run(
+                    [*pairs([tile16(c, i, False) for i in each]), [tile4_first(c, True)]]
+                    + [[tile4(c, n)] for n in range(1, nq // 4)]
+                )
+
+    w_away.start()
 
     with scope("i_t1"):
-        @pl.when(has_next)
-        def _():
-            copy_x().start()
-
-        run([tile1_part(1)])
-
-        @pl.loop(0, (nq - 1) // 5)
-        def _(i):
-            run([tile1(1 + 5 * i + n) for n in range(5)])
+        run([[tile1(h)] for h in range(1, nq)])
 
         @pl.when(has_prev)
         def _():
-            drain(kv.at[:, 0], r_x)
-            run([tile1_part(0)])
+            drain(kv.at[:, :own0], r_x)
+            run([[tile1(0)], *[[tilex(c, i) for i in range(PIECE // 16)] for c in range(CHUNKS)]])
+
+        @pl.when(jnp.logical_not(has_prev))
+        def _():
+            run([[tile1(0)]])
 
     eye = jnp.where(iota(flat, 0) == iota(flat, 1), 1.0, 0.0).astype(BF16)
     upper = iota(flat, 0) < HD
 
-    def finish(c, merge):
-        if merge:
-            stats = oin[c, nq * half :].astype(F32)
-        for g in range(nq // eight):
-            at = slice(g * eight, (g + 1) * eight)
-            a = acc[c, at]
+    def merge(c, g, extra=False):
+        at = slice(g * eight, (g + 1) * eight)
+        parts = []
+        for sums, tops in ((acc1, top1), (acc4, top4), (acc16, top16), (accx, topx)):
+            if sums is accx and not extra:
+                continue
+            a = sums[c] if sums is accx else sums[c, at]
+            t = tops[c] if sums is accx else tops[c, at]
             z = pltpu.roll(a, HD, 2)
-            num = jnp.where(low_h, z[:, :half], a[:, half:]).reshape(flat)
-            den = jnp.where(low_h, a[:, :half], z[:, half:]).reshape(flat)
-            if merge:
-                def spread(j):
-                    both = jnp.where(
-                        upper,
-                        jnp.broadcast_to(stats[8 * g + j : 8 * g + j + 1], flat),
-                        jnp.broadcast_to(stats[8 * g + j + 1 : 8 * g + j + 2], flat),
-                    )
-                    return lax.dot_general(eye, both.astype(BF16), NT, preferred_element_type=F32)
-
-                t = top[c, at]
-                t = jnp.where(low_h, t[:, :half], t[:, half:]).reshape(flat)
-                t_old = spread(0)
-                t_new = jnp.maximum(t, t_old)
-                mine = jnp.exp(t - t_new)
-                theirs = jnp.exp(t_old - t_new)
-                num = num * mine + oin[c, g * BACK : (g + 1) * BACK].astype(F32) * theirs
-                den = den * mine + (spread(2) + spread(4)) * theirs
-            rs[c, at] = (num / den).astype(BF16).reshape(eight, half, LANES)
+            parts.append((
+                jnp.where(low_h, z[:, :half], a[:, half:]),
+                jnp.where(low_h, a[:, :half], z[:, half:]),
+                jnp.where(low_h, t[:, :half], t[:, half:]),
+            ))
+        t = functools.reduce(jnp.maximum, [part[2] for part in parts])
+        scales = [jnp.exp(part[2] - t) for part in parts]
+        num = sum(part[0] * scale for part, scale in zip(parts, scales))
+        den = sum(part[1] * scale for part, scale in zip(parts, scales))
+        return num, den, t
+
+    def finish(c, g, num, den):
+        rs[c, g * eight : (g + 1) * eight] = (num / den).astype(BF16).reshape(eight, half, LANES)
+
+    def finish_old(c):
+        stats = oin[c, BACK:].astype(F32)
+
+        def spread(j):
+            both = jnp.where(
+                upper,
+                jnp.broadcast_to(stats[j : j + 1], flat),
+                jnp.broadcast_to(stats[j + 1 : j + 2], flat),
+            )
+            return lax.dot_general(eye, both.astype(BF16), NT, preferred_element_type=F32)
+
+        t = pt[c]
+        t_old = spread(0)
+        t_new = jnp.maximum(t, t_old)
+        mine = jnp.exp(t - t_new)
+        theirs = jnp.exp(t_old - t_new)
+        finish(
+            c, 0, pn[c] * mine + oin[c, :BACK].astype(F32) * theirs,
+            pd[c] * mine + (spread(2) + spread(4)) * theirs,
+        )
 
     def copy_ret(c, n):
         return remote(
@@ -402,36 +476,64 @@
             target(base + n // tp_count, lax.rem(n, tp_count)),
         )
 
+    def give(c, g):
+        for o in quad:
+            dest = g * hb + lax.rem(mate(o), hb)
+            copy_ret(c, dest * tp_count + tp_count - 1 - tp).start()
+            if o:
+                copy_ret(c, dest * tp_count + tp).start()
+            else:
+                @pl.when(dest != me)
+                def _():
+                    copy_ret(c, dest * tp_count + tp).start()
+
+    groups = range(nq // eight)
+
     with scope("o_finish"):
-        @pl.loop(0, CHUNKS)
-        def _(c):
-            @pl.when(has_prev)
-            def _():
+        @pl.when(has_prev)
+        def _():
+            for c in range(CHUNKS):
+                finish(c, 1, *merge(c, 1, True)[:2])
+            for c in range(CHUNKS):
+                give(c, 1)
+            for c in range(CHUNKS):
+                num, den, t = merge(c, 0)
+                pn[c] = num.reshape(flat)
+                pd[c] = den.reshape(flat)
+                pt[c] = t.reshape(flat)
+
+            @pl.loop(0, CHUNKS)
+            def _(c):
                 drain(oin.at[c], r_o.at[c])
-                finish(c, True)
-
-            @pl.when(jnp.logical_not(has_prev))
-            def _():
-                finish(c, False)
-
-            for o in far + [0]:
-                copy_ret(c, mate(o) * tp_count + tp_count - 1 - tp).start()
-                if o:
-                    copy_ret(c, mate(o) * tp_count + tp).start()
-            rr[c, head] = rs[c, seat]
+                finish_old(c)
+                give(c, 0)
+
+        @pl.when(jnp.logical_not(has_prev))
+        def _():
+            for c in range(CHUNKS):
+                for g in groups:
+                    finish(c, g, *merge(c, g)[:2])
+            for c in range(CHUNKS):
+                for g in groups:
+                    give(c, g)
+
+        rr[:, head] = rs[:, seat]
 
     with scope("q_sendwait"):
         drain(kvs.at[:, : G - 1], s_kv)
         drain(qs.at[:, : G - 1], s_q)
 
-        @pl.when(has_prev)
+        @pl.when(jnp.logical_and(has_prev, me < hb))
         def _():
             drain(qs, s_qb)
 
         @pl.when(has_next)
         def _():
             drain(ob, s_o)
-            drain(kv.at[:, 0], s_x)
+
+        @pl.when(jnp.logical_and(has_next, me >= hb))
+        def _():
+            drain(kvs, s_x)
 
         w_local.wait()
         w_away.wait_send()
@@ -506,21 +608,20 @@
             pltpu.VMEM((CHUNKS, G, PIECE, LANES), BF16),
             pltpu.VMEM((CHUNKS, G, halves, PIECE, LANES), BF16),
             pltpu.VMEM((CHUNKS, G, PIECE, LANES), BF16),
-            pltpu.VMEM((CHUNKS, 1 + nq, PIECE, LANES), BF16),
+            pltpu.VMEM((CHUNKS, nq + nq // 2, PIECE, LANES), BF16),
             pltpu.VMEM((nq, PIECE, LANES), F32),
             pltpu.VMEM((CHUNKS, nq, PIECE, LANES), BF16),
-            pltpu.VMEM((nq, PIECE, LANES), F32),
-            pltpu.VMEM((CHUNKS, nq, PIECE, LANES), F32),
-            pltpu.VMEM((CHUNKS, nq, PIECE, LANES), F32),
-            pltpu.VMEM((CHUNKS, G, PIECE, LANES), BF16),
-            pltpu.VMEM((nq, PIECE, LANES), F32),
-            pltpu.VMEM((nq, PIECE, LANES), F32),
-            pltpu.VMEM((nq, PIECE, LANES), F32),
-            pltpu.VMEM((CHUNKS, nq * PIECE // 2 + 16, LANES), BF16),
-            pltpu.VMEM((CHUNKS, nq * PIECE // 2 + 16, LANES), BF16),
+            *[pltpu.VMEM((CHUNKS, nq, PIECE, LANES), F32)] * 7,
+            *[pltpu.VMEM((CHUNKS, nq // 2, PIECE, LANES), F32)] * 2,
+            pltpu.VMEM((CHUNKS, G // 2, PIECE, LANES), BF16),
+            *[pltpu.VMEM((nq // 2, PIECE, LANES), F32)] * 3,
+            *[pltpu.VMEM((4, PIECE, LANES), F32)] * 2,
+            *[pltpu.VMEM((CHUNKS, BACK + 16, LANES), BF16)] * 2,
+            *[pltpu.VMEM((CHUNKS, BACK, LANES), F32)] * 3,
             pltpu.VMEM((BACK, 2 * BACK), F32),
             pltpu.VMEM((BACK, 2 * BACK), F32),
             pltpu.VMEM((BACK, 2 * BACK), F32),
+            pltpu.VMEM((BACK, BACK), F32),
             pltpu.VMEM((tp_count,) + out_weight.shape, BF16),
             pltpu.VMEM((CHUNKS, seats, PIECE // 2, LANES), BF16),
             pltpu.VMEM((CHUNKS, seats, PIECE // 2, LANES), BF16),

time: 35.7 us -> 31.6 us (0.89); the launches traced: 35.2 us -> 31.5 us
  Pallas kernels: 34.4 us -> 30.7 us
    pallas_call x1, Pallas kernels: 34.4 us -> 30.7 us  [per_device(): pl.pallas_call(functools.partial(kernel, G, ngroups, tp_count), out_shape...]
where the time goes in v2:
time: 31.6 us; the launch traced here: 31.5 us
  Pallas kernels  30.7 us (97%)
  local copies, waits for them, and re-layouts  0.8 us (3%)
    pallas_call x1, Pallas kernels, per_device(): pl.pallas_call(functools.partial(kernel, G, ngroups, tp_count), out_shape...  30.7 us
    unnamed x1, local copies, waits for them, and re-layouts  0.8 us

profile of v2, /device:TPU:17, one launch (start us, length us, event | category | flops | bytes accessed | tf_op | source)
XLA Modules:
  0.0 31.5 jit_solution(11496152138488573277)
XLA Ops:
  0.0 30.7 %shard_map.73 = bf16[128,2048]{1,0:T(8,128)(2,1)S(1)} custom-call(bf16[256,512]{1,0:T(8,128)(2,1)} %q_hbm.1, bf16[256,512]{1,0:T(8,128)(2,1)} %k_hbm.1, bf16[256,512]{1,0:T(8,128)(2,1)} %v_hbm.1, f32[256,128]{1,0:T(8,128)} %constant.6.clone.cosb_hbm, f32[256,128]{1,0:T(8,128)} %constant.7.clone.sinb_hbm, f32[8,128]{1,0:T(8,128)} %constant.8.clone.inv_hbm, ...), custom_call_target="tpu_custom_call" | custom-call | tf_op jit(solution)/shard_map/pallas_call | solution.py:596
  30.7 0.8 %copy.9 = bf16[128,2048]{1,0:T(8,128)(2,1)} copy(bf16[128,2048]{1,0:T(8,128)(2,1)S(1)} %shard_map.73) | data formatting | bytes 1048576

commit v3 on v2

--- a/solution.py
+++ b/solution.py
@@ -18,6 +18,8 @@
 LANES = 2 * HD
 CHUNKS = 4
 PIECE = BACK // CHUNKS
+STATS = 16
+EARLY = 4
 NT = (((1,), (1,)), ((), ()))
 
 
@@ -34,7 +36,7 @@
     q_hbm, k_hbm, v_hbm, cosb_hbm, sinb_hbm, inv_hbm, w_ref, out_ref,
     q_ref, k_ref, v_ref, cosb_ref, sinb_ref, inv_ref, qs, kvs, qr, kv, kvf, q2, q2f,
     acc1, top1, acc4, top4, acc16, top16, accx, topx, qb, qbf, accb, topb, accb4, topb4, ob, oin, pn, pd, pt, b1_ref, b4_ref, b16_ref, bx_ref, wbuf, rs, rr, mx,
-    s_kv, s_q, s_qb, s_x, s_o, s_ret, r_kv, r_q, r_qb, r_x, r_o, r_ret, w_sem, in_sem,
+    s_kv, s_q, s_qb, s_x, s_y, s_o, s_ret, r_kv, r_q, r_qb, r_x, r_o, r_ret, w_sem, in_sem,
 ):
     loads = [
         pltpu.make_async_copy(source, dest, in_sem.at[n])
@@ -61,6 +63,8 @@
     hb = G // 2
     nh = nq // 2
     own0 = nh
+    lower = me < hb
+    upper = me >= hb
 
     def target(s, t):
         return {"sp": s, "tp": t}
@@ -186,6 +190,11 @@
             qs.at[c, dest], qb.at[c, me], s_qb, r_qb.at[c], target(base - G + dest, tp)
         )
 
+    def copy_y(c, dest):
+        return remote(
+            kvs.at[c, dest, halves - 1], kv.at[c, own0 - 1], s_y, r_x, target(base + G + dest, tp)
+        )
+
     def copy_x(c, dest):
         return remote(
             kvs.at[c, dest], kv.at[c, pl.ds(halves * (me - hb), halves)],
@@ -205,20 +214,33 @@
     def mate(o):
         return sum((((me // b + o // b) % 2) * b for b in bits), 0)
 
+    def send_back(c):
+        @pl.when(jnp.logical_and(has_prev, lower))
+        def _():
+            for o in [*far, 0]:
+                copy_qb(c, mate(o)).start()
+
+        @pl.when(jnp.logical_and(has_prev, upper))
+        def _():
+            for o in quad:
+                copy_qb(c, hb + lax.rem(mate(o), hb)).start()
+
     with scope("e_issue"):
-        @pl.when(jnp.logical_and(has_next, me >= hb))
-        def _():
-            for part in (0, hb):
-                for c in range(CHUNKS):
-                    for o in quad:
-                        copy_x(c, part + lax.rem(mate(o), hb)).start()
+        @pl.when(jnp.logical_and(has_next, upper))
+        def _():
+            for c in range(CHUNKS):
+                for o in quad:
+                    copy_x(c, lax.rem(mate(o), hb)).start()
+
+        @pl.when(jnp.logical_and(has_next, me == G - 1))
+        def _():
+            for c in range(CHUNKS):
+                for o in quad:
+                    copy_y(c, hb + lax.rem(mate(o), hb)).start()
 
         for c in range(CHUNKS):
-            @pl.when(jnp.logical_and(has_prev, me < hb))
-            def _():
-                for o in [*far, 0]:
-                    copy_qb(c, mate(o)).start()
-
+            if c < EARLY:
+                send_back(c)
             for o in far:
                 copy_q(c, mate(o)).start()
                 copy_kv(c, mate(o)).start()
@@ -229,8 +251,8 @@
 
     low_p = low[:PIECE]
 
-    def unpack(ref, c, wide, narrow=None):
-        for s in range(ref.shape[1]):
+    def unpack(ref, c, sources, wide, narrow=None):
+        for s in range(sources):
             x = ref[c, s].astype(F32)
             a = jnp.where(low_p, x, 0.0)
             b = jnp.where(low_p, pltpu.roll(x, HD, 1), 0.0)
@@ -313,16 +335,16 @@
             b4_ref[:, :BACK], ((accb4, topb4, (every,)),),
         )
 
-    def tile16(c, i, both):
+    def tile16(c, i, olds):
         rows = slice(8 * i, 8 * i + 8)
         q = q2f[c, :, rows].reshape(BACK, LANES).astype(BF16)
         b = b16_ref[:, BACK:]
         places = ((acc16, top16, (c, every, rows)),)
-        if both:
-            old = qbf[:, rows].reshape(-1, LANES).astype(BF16)
+        if olds:
+            old = qbf[:olds, rows].reshape(-1, LANES).astype(BF16)
             q = jnp.concatenate([q, old], axis=0)
             b = jnp.concatenate([b, b16_ref[: old.shape[0], :BACK]], axis=0)
-            places = (*places, (accb, topb, (every, rows)))
+            places = (*places, (accb, topb, (slice(0, olds), rows)))
         return (q, kvf[:, rows].reshape(BACK, LANES).astype(BF16), b, places)
 
     def tilex(c, i):
@@ -342,20 +364,20 @@
     def rounded(x):
         return x.astype(BF16).astype(F32)
 
-    def send_old(c):
+    def send_old(c, olds):
         t4, t16 = topb4[...], topb[:4]
         t = jnp.maximum(t4, t16)
         accb[:4] = accb[:4] * jnp.exp(t16 - t) + accb4[...] * jnp.exp(t4 - t)
         topb[:4] = t
-        stats = jnp.zeros((2 * 8, LANES), F32)
-        for g in range(1):
+        stats = jnp.zeros((STATS, LANES), F32)
+        for g in range(olds // eight):
             at = slice(g * eight, (g + 1) * eight)
             t = topb[at]
             mark = rounded(t)
             a = accb[at] * jnp.exp(t - mark)
             z = pltpu.roll(a, HD, 2)
             lo, hi = a[:, :half], a[:, half:]
-            ob[c, g * BACK : (g + 1) * BACK] = (
+            ob[c, STATS + g * BACK : STATS + (g + 1) * BACK] = (
                 jnp.where(low_h, z[:, :half], hi).astype(BF16).reshape(flat)
             )
             columns = mark[:, half:]
@@ -364,18 +386,28 @@
             columns = jnp.where(lane_h == 3, rounded(hi), columns)
             columns = jnp.where(lane_h == 4, lo - rounded(lo), columns)
             columns = jnp.where(lane_h == 5, hi - rounded(hi), columns)
-            pick = (iota((2 * 8, LANES), 0) - 8 * g == iota((2 * 8, LANES), 1)) & (
-                iota((2 * 8, LANES), 1) < 6
+            pick = (iota((STATS, LANES), 0) - 8 * g == iota((STATS, LANES), 1)) & (
+                iota((STATS, LANES), 1) < 6
             )
             stats = stats + lax.dot_general(
                 jnp.where(pick, 1.0, 0.0).astype(BF16), columns.astype(BF16).reshape(flat), NT,
                 preferred_element_type=F32,
             )
-        ob[c, BACK:] = stats.astype(BF16)
-        copy_o(c).start()
-
-    def copy_o(c):
-        return remote(ob.at[c], oin.at[c], s_o, r_o.at[c], target(sp + G, tp))
+        ob[c, :STATS] = stats.astype(BF16)
+        copy_o(c, olds).start()
+
+    def old_rows(olds):
+        return slice(0, STATS + olds * half)
+
+    def copy_o(c, olds):
+        at = old_rows(olds)
+        return remote(ob.at[c, at], oin.at[c, at], s_o, r_o.at[c], target(sp + G, tp))
+
+    def blend(c):
+        t4, t16 = top4[c], top16[c]
+        t = jnp.maximum(t4, t16)
+        acc16[c] = acc4[c] * jnp.exp(t4 - t) + acc16[c] * jnp.exp(t16 - t)
+        top16[c] = t
 
     missing = jnp.logical_and(col < BACK, group == 0)
 
@@ -390,84 +422,93 @@
             drain(kv.at[c, own0 : own0 + halves * (G - 1)], r_kv.at[c])
             kvf[...] = kv[c, own0:].astype(F32)
 
-            @pl.when(has_next)
-            def _():
-                drain(qb.at[c], r_qb.at[c])
-                unpack(qb, c, qbf)
-                unpack(qr, c, q2f.at[c], q2)
+
+            def serve(olds):
+                if olds:
+                    drain(qb.at[c, : olds // halves], r_qb.at[c])
+                    unpack(qb, c, olds // halves, qbf)
+                unpack(qr, c, G, q2f.at[c], q2)
+                four = [tile4_old(c), tile4_first(c, False)] if olds else [tile4_first(c, True)]
                 run(
-                    [*pairs([tile16(c, i, True) for i in each]), [tile4_old(c), tile4_first(c, False)]]
+                    [*pairs([tile16(c, i, olds) for i in each]), four]
                     + [[tile4(c, n)] for n in range(1, nq // 4)]
                 )
-                send_old(c)
+                if olds:
+                    send_old(c, olds)
+                blend(c)
+
+            @pl.when(jnp.logical_and(has_next, lower))
+            def _():
+                serve(nh)
+
+            @pl.when(jnp.logical_and(has_next, upper))
+            def _():
+                serve(nq)
 
             @pl.when(jnp.logical_not(has_next))
             def _():
-                unpack(qr, c, q2f.at[c], q2)
-                run(
-                    [*pairs([tile16(c, i, False) for i in each]), [tile4_first(c, True)]]
-                    + [[tile4(c, n)] for n in range(1, nq // 4)]
-                )
+                serve(0)
 
     w_away.start()
 
     with scope("i_t1"):
         run([[tile1(h)] for h in range(1, nq)])
 
-        @pl.when(has_prev)
+        @pl.when(jnp.logical_and(has_prev, lower))
         def _():
             drain(kv.at[:, :own0], r_x)
             run([[tile1(0)], *[[tilex(c, i) for i in range(PIECE // 16)] for c in range(CHUNKS)]])
 
+        @pl.when(jnp.logical_and(has_prev, upper))
+        def _():
+            drain(kv.at[:, own0 - 1], r_x)
+            run([[tile1(0)]])
+
         @pl.when(jnp.logical_not(has_prev))
         def _():
             run([[tile1(0)]])
 
     eye = jnp.where(iota(flat, 0) == iota(flat, 1), 1.0, 0.0).astype(BF16)
-    upper = iota(flat, 0) < HD
+    top_rows = iota(flat, 0) < HD
 
     def merge(c, g, extra=False):
         at = slice(g * eight, (g + 1) * eight)
-        parts = []
-        for sums, tops in ((acc1, top1), (acc4, top4), (acc16, top16), (accx, topx)):
-            if sums is accx and not extra:
-                continue
-            a = sums[c] if sums is accx else sums[c, at]
-            t = tops[c] if sums is accx else tops[c, at]
-            z = pltpu.roll(a, HD, 2)
-            parts.append((
-                jnp.where(low_h, z[:, :half], a[:, half:]),
-                jnp.where(low_h, a[:, :half], z[:, half:]),
-                jnp.where(low_h, t[:, :half], t[:, half:]),
-            ))
-        t = functools.reduce(jnp.maximum, [part[2] for part in parts])
-        scales = [jnp.exp(part[2] - t) for part in parts]
-        num = sum(part[0] * scale for part, scale in zip(parts, scales))
-        den = sum(part[1] * scale for part, scale in zip(parts, scales))
-        return num, den, t
+        parts = [(acc1[c, at], top1[c, at]), (acc16[c, at], top16[c, at])]
+        if extra:
+            parts.append((accx[c], topx[c]))
+        t = functools.reduce(jnp.maximum, [part[1] for part in parts])
+        a = sum(part[0] * jnp.exp(part[1] - t) for part in parts)
+        z = pltpu.roll(a, HD, 2)
+        return (
+            jnp.where(low_h, z[:, :half], a[:, half:]),
+            jnp.where(low_h, a[:, :half], z[:, half:]),
+            jnp.where(low_h, t[:, :half], t[:, half:]),
+        )
 
     def finish(c, g, num, den):
         rs[c, g * eight : (g + 1) * eight] = (num / den).astype(BF16).reshape(eight, half, LANES)
 
-    def finish_old(c):
-        stats = oin[c, BACK:].astype(F32)
+    def finish_old(c, g):
+        stats = oin[c, :STATS].astype(F32)
 
         def spread(j):
+            at = 8 * g + j
             both = jnp.where(
-                upper,
-                jnp.broadcast_to(stats[j : j + 1], flat),
-                jnp.broadcast_to(stats[j + 1 : j + 2], flat),
+                top_rows,
+                jnp.broadcast_to(stats[at : at + 1], flat),
+                jnp.broadcast_to(stats[at + 1 : at + 2], flat),
             )
             return lax.dot_general(eye, both.astype(BF16), NT, preferred_element_type=F32)
 
-        t = pt[c]
+        t = pt[c, g]
         t_old = spread(0)
         t_new = jnp.maximum(t, t_old)
         mine = jnp.exp(t - t_new)
         theirs = jnp.exp(t_old - t_new)
+        old = oin[c, STATS + g * BACK : STATS + (g + 1) * BACK].astype(F32)
         finish(
-            c, 0, pn[c] * mine + oin[c, :BACK].astype(F32) * theirs,
-            pd[c] * mine + (spread(2) + spread(4)) * theirs,
+            c, g, pn[c, g] * mine + old * theirs,
+            pd[c, g] * mine + (spread(2) + spread(4)) * theirs,
         )
 
     def copy_ret(c, n):
@@ -489,24 +530,37 @@
 
     groups = range(nq // eight)
 
+    def close(olds, late):
+        for c in range(CHUNKS):
+            for g in late:
+                num, den, t = merge(c, g)
+                pn[c, g] = num.reshape(flat)
+                pd[c, g] = den.reshape(flat)
+                pt[c, g] = t.reshape(flat)
+
+        @pl.loop(0, CHUNKS // 2)
+        def _(i):
+            for c in (2 * i, 2 * i + 1):
+                drain(oin.at[c, old_rows(olds)], r_o.at[c])
+            for c in (2 * i, 2 * i + 1):
+                for g in late:
+                    finish_old(c, g)
+            for c in (2 * i, 2 * i + 1):
+                for g in late:
+                    give(c, g)
+
     with scope("o_finish"):
-        @pl.when(has_prev)
+        @pl.when(jnp.logical_and(has_prev, lower))
         def _():
             for c in range(CHUNKS):
                 finish(c, 1, *merge(c, 1, True)[:2])
             for c in range(CHUNKS):
                 give(c, 1)
-            for c in range(CHUNKS):
-                num, den, t = merge(c, 0)
-                pn[c] = num.reshape(flat)
-                pd[c] = den.reshape(flat)
-                pt[c] = t.reshape(flat)
-
-            @pl.loop(0, CHUNKS)
-            def _(c):
-                drain(oin.at[c], r_o.at[c])
-                finish_old(c)
-                give(c, 0)
+            close(nh, (0,))
+
+        @pl.when(jnp.logical_and(has_prev, upper))
+        def _():
+            close(nq, (0, 1))
 
         @pl.when(jnp.logical_not(has_prev))
         def _():
@@ -523,17 +577,26 @@
         drain(kvs.at[:, : G - 1], s_kv)
         drain(qs.at[:, : G - 1], s_q)
 
-        @pl.when(jnp.logical_and(has_prev, me < hb))
+        @pl.when(jnp.logical_and(has_prev, lower))
         def _():
             drain(qs, s_qb)
 
-        @pl.when(has_next)
+        @pl.when(jnp.logical_and(has_prev, upper))
+        def _():
+            drain(qs.at[:, :hb], s_qb)
+
+        @pl.when(jnp.logical_and(has_next, lower))
+        def _():
+            drain(ob.at[:, old_rows(nh)], s_o)
+
+        @pl.when(jnp.logical_and(has_next, upper))
         def _():
             drain(ob, s_o)
-
-        @pl.when(jnp.logical_and(has_next, me >= hb))
-        def _():
-            drain(kvs, s_x)
+            drain(kvs.at[:, :hb], s_x)
+
+        @pl.when(jnp.logical_and(has_next, me == G - 1))
+        def _():
+            drain(kvs.at[:, :hb, halves - 1], s_y)
 
         w_local.wait()
         w_away.wait_send()
@@ -561,7 +624,7 @@
             ).astype(BF16)
 
     width = wbuf.shape[1]
-    step = 512
+    step = 2048
 
     with scope("u_proj"):
         @pl.loop(0, out_ref.shape[1] // step)
@@ -613,11 +676,11 @@
             pltpu.VMEM((CHUNKS, nq, PIECE, LANES), BF16),
             *[pltpu.VMEM((CHUNKS, nq, PIECE, LANES), F32)] * 7,
             *[pltpu.VMEM((CHUNKS, nq // 2, PIECE, LANES), F32)] * 2,
-            pltpu.VMEM((CHUNKS, G // 2, PIECE, LANES), BF16),
-            *[pltpu.VMEM((nq // 2, PIECE, LANES), F32)] * 3,
+            pltpu.VMEM((CHUNKS, G, PIECE, LANES), BF16),
+            *[pltpu.VMEM((nq, PIECE, LANES), F32)] * 3,
             *[pltpu.VMEM((4, PIECE, LANES), F32)] * 2,
-            *[pltpu.VMEM((CHUNKS, BACK + 16, LANES), BF16)] * 2,
-            *[pltpu.VMEM((CHUNKS, BACK, LANES), F32)] * 3,
+            *[pltpu.VMEM((CHUNKS, STATS + nq * PIECE // 2, LANES), BF16)] * 2,
+            *[pltpu.VMEM((CHUNKS, nq * PIECE // (2 * BACK), BACK, LANES), F32)] * 3,
             pltpu.VMEM((BACK, 2 * BACK), F32),
             pltpu.VMEM((BACK, 2 * BACK), F32),
             pltpu.VMEM((BACK, 2 * BACK), F32),
@@ -626,7 +689,7 @@
             pltpu.VMEM((CHUNKS, seats, PIECE // 2, LANES), BF16),
             pltpu.VMEM((CHUNKS, seats, PIECE // 2, LANES), BF16),
             pltpu.VMEM((BACK, seats * HD), BF16),
-            dma, dma, dma, dma, dma, dma,
+            dma, dma, dma, dma, dma, dma, dma,
             dma((CHUNKS,)), dma((CHUNKS,)), dma((CHUNKS,)), dma, dma((CHUNKS,)), dma,
             dma((3,)), dma((6,)),
         ],

time: 31.6 us -> 29.9 us (0.946)
  Pallas kernels: 30.7 us -> 28.9 us
    pallas_call x1, Pallas kernels: 30.7 us -> 28.9 us  [per_device(): pl.pallas_call(functools.partial(kernel, G, ngroups, tp_count), out_shape...]
where the time goes in v3:
time: 29.9 us; the launch traced here: 29.7 us
  Pallas kernels  28.9 us (97%)
  local copies, waits for them, and re-layouts  0.8 us (3%)
    pallas_call x1, Pallas kernels, per_device(): pl.pallas_call(functools.partial(kernel, G, ngroups, tp_count), out_shape...  28.9 us
    unnamed x1, local copies, waits for them, and re-layouts  0.8 us

profile of v3, /device:TPU:17, one launch (start us, length us, event | category | flops | bytes accessed | tf_op | source)
XLA Modules:
  0.0 29.7 jit_solution(15406147368882010992)
XLA Ops:
  0.0 28.9 %shard_map.73 = bf16[128,2048]{1,0:T(8,128)(2,1)S(1)} custom-call(bf16[256,512]{1,0:T(8,128)(2,1)} %q_hbm.1, bf16[256,512]{1,0:T(8,128)(2,1)} %k_hbm.1, bf16[256,512]{1,0:T(8,128)(2,1)} %v_hbm.1, f32[256,128]{1,0:T(8,128)} %constant.6.clone.cosb_hbm, f32[256,128]{1,0:T(8,128)} %constant.7.clone.sinb_hbm, f32[8,128]{1,0:T(8,128)} %constant.8.clone.inv_hbm, ...), custom_call_target="tpu_custom_call" | custom-call | tf_op jit(solution)/shard_map/pallas_call | solution.py:659
  29.0 0.8 %copy.9 = bf16[128,2048]{1,0:T(8,128)(2,1)} copy(bf16[128,2048]{1,0:T(8,128)(2,1)S(1)} %shard_map.73) | data formatting | bytes 1048576

commit v4 on v3

--- a/solution.py
+++ b/solution.py
@@ -19,7 +19,6 @@
 CHUNKS = 4
 PIECE = BACK // CHUNKS
 STATS = 16
-EARLY = 4
 NT = (((1,), (1,)), ((), ()))
 
 
@@ -239,8 +238,7 @@
                     copy_y(c, hb + lax.rem(mate(o), hb)).start()
 
         for c in range(CHUNKS):
-            if c < EARLY:
-                send_back(c)
+            send_back(c)
             for o in far:
                 copy_q(c, mate(o)).start()
                 copy_kv(c, mate(o)).start()
@@ -421,6 +419,7 @@
             drain(qr.at[c, : G - 1], r_q.at[c])
             drain(kv.at[c, own0 : own0 + halves * (G - 1)], r_kv.at[c])
             kvf[...] = kv[c, own0:].astype(F32)
+            pl.when(c == 1)(w_away.start)
 
 
             def serve(olds):
@@ -449,24 +448,26 @@
             def _():
                 serve(0)
 
-    w_away.start()
 
     with scope("i_t1"):
-        run([[tile1(h)] for h in range(1, nq)])
-
-        @pl.when(jnp.logical_and(has_prev, lower))
+        takes = jnp.logical_and(has_prev, lower)
+        ones_tiles = range(nq)
+
+        @pl.when(takes)
         def _():
             drain(kv.at[:, :own0], r_x)
-            run([[tile1(0)], *[[tilex(c, i) for i in range(PIECE // 16)] for c in range(CHUNKS)]])
+            run(
+                [[tile1(h)] for h in ones_tiles]
+                + [[tilex(c, i) for i in range(PIECE // 16)] for c in range(CHUNKS)]
+            )
 
         @pl.when(jnp.logical_and(has_prev, upper))
         def _():
             drain(kv.at[:, own0 - 1], r_x)
-            run([[tile1(0)]])
-
-        @pl.when(jnp.logical_not(has_prev))
-        def _():
-            run([[tile1(0)]])
+
+        @pl.when(jnp.logical_not(takes))
+        def _():
+            run([[tile1(h)] for h in ones_tiles])
 
     eye = jnp.where(iota(flat, 0) == iota(flat, 1), 1.0, 0.0).astype(BF16)
     top_rows = iota(flat, 0) < HD
@@ -538,16 +539,13 @@
                 pd[c, g] = den.reshape(flat)
                 pt[c, g] = t.reshape(flat)
 
-        @pl.loop(0, CHUNKS // 2)
-        def _(i):
-            for c in (2 * i, 2 * i + 1):
-                drain(oin.at[c, old_rows(olds)], r_o.at[c])
-            for c in (2 * i, 2 * i + 1):
-                for g in late:
-                    finish_old(c, g)
-            for c in (2 * i, 2 * i + 1):
-                for g in late:
-                    give(c, g)
+        @pl.loop(0, CHUNKS)
+        def _(c):
+            drain(oin.at[c, old_rows(olds)], r_o.at[c])
+            for g in late:
+                finish_old(c, g)
+            for g in late:
+                give(c, g)
 
     with scope("o_finish"):
         @pl.when(jnp.logical_and(has_prev, lower))
@@ -624,7 +622,7 @@
             ).astype(BF16)
 
     width = wbuf.shape[1]
-    step = 2048
+    step = out_ref.shape[1]
 
     with scope("u_proj"):
         @pl.loop(0, out_ref.shape[1] // step)

time: 29.9 us -> 29.5 us (0.987)
  Pallas kernels: 28.9 us -> 28.4 us
    pallas_call x1, Pallas kernels: 28.9 us -> 28.4 us  [per_device(): pl.pallas_call(functools.partial(kernel, G, ngroups, tp_count), out_shape...]
where the time goes in v4:
time: 29.5 us; the launch traced here: 29.2 us
  Pallas kernels  28.4 us (96%)
  local copies, waits for them, and re-layouts  0.8 us (3%)
    pallas_call x1, Pallas kernels, per_device(): pl.pallas_call(functools.partial(kernel, G, ngroups, tp_count), out_shape...  28.4 us
    unnamed x1, local copies, waits for them, and re-layouts  0.8 us

profile of v4, /device:TPU:17, one launch (start us, length us, event | category | flops | bytes accessed | tf_op | source)
XLA Modules:
  0.0 29.2 jit_solution(8685415697897091608)
XLA Ops:
  0.0 28.4 %shard_map.73 = bf16[128,2048]{1,0:T(8,128)(2,1)S(1)} custom-call(bf16[256,512]{1,0:T(8,128)(2,1)} %q_hbm.1, bf16[256,512]{1,0:T(8,128)(2,1)} %k_hbm.1, bf16[256,512]{1,0:T(8,128)(2,1)} %v_hbm.1, f32[256,128]{1,0:T(8,128)} %constant.6.clone.cosb_hbm, f32[256,128]{1,0:T(8,128)} %constant.7.clone.sinb_hbm, f32[8,128]{1,0:T(8,128)} %constant.8.clone.inv_hbm, ...), custom_call_target="tpu_custom_call" | custom-call | tf_op jit(solution)/shard_map/pallas_call | solution.py:657
  28.4 0.8 %copy.9 = bf16[128,2048]{1,0:T(8,128)(2,1)} copy(bf16[128,2048]{1,0:T(8,128)(2,1)S(1)} %shard_map.73) | data formatting | bytes 1048576

commit v5 on v4

--- a/solution.py
+++ b/solution.py
@@ -562,12 +562,13 @@
 
         @pl.when(jnp.logical_not(has_prev))
         def _():
-            for c in range(CHUNKS):
-                for g in groups:
-                    finish(c, g, *merge(c, g)[:2])
-            for c in range(CHUNKS):
-                for g in groups:
-                    give(c, g)
+            for part in (range(CHUNKS // 2), range(CHUNKS // 2, CHUNKS)):
+                for c in part:
+                    for g in groups:
+                        finish(c, g, *merge(c, g)[:2])
+                for c in part:
+                    for g in groups:
+                        give(c, g)
 
         rr[:, head] = rs[:, seat]
 

time: 29.5 us -> 29.3 us (level)
  no operation moved by 1% of the time
where the time goes in v5:
time: 29.3 us; the launch traced here: 29.2 us
  Pallas kernels  28.4 us (97%)
  local copies, waits for them, and re-layouts  0.8 us (3%)
    pallas_call x1, Pallas kernels, per_device(): pl.pallas_call(functools.partial(kernel, G, ngroups, tp_count), out_shape...  28.4 us
    unnamed x1, local copies, waits for them, and re-layouts  0.8 us

profile of v5, /device:TPU:17, one launch (start us, length us, event | category | flops | bytes accessed | tf_op | source)
XLA Modules:
  0.0 29.2 jit_solution(15143365623310388697)
XLA Ops:
  0.0 28.4 %shard_map.73 = bf16[128,2048]{1,0:T(8,128)(2,1)S(1)} custom-call(bf16[256,512]{1,0:T(8,128)(2,1)} %q_hbm.1, bf16[256,512]{1,0:T(8,128)(2,1)} %k_hbm.1, bf16[256,512]{1,0:T(8,128)(2,1)} %v_hbm.1, f32[256,128]{1,0:T(8,128)} %constant.6.clone.cosb_hbm, f32[256,128]{1,0:T(8,128)} %constant.7.clone.sinb_hbm, f32[8,128]{1,0:T(8,128)} %constant.8.clone.inv_hbm, ...), custom_call_target="tpu_custom_call" | custom-call | tf_op jit(solution)/shard_map/pallas_call | solution.py:658
  28.4 0.8 %copy.9 = bf16[128,2048]{1,0:T(8,128)(2,1)} copy(bf16[128,2048]{1,0:T(8,128)(2,1)S(1)} %shard_map.73) | data formatting | bytes 1048576
